TPU v7x, 32 devices: a whole 2x2x4 slice. The times are simulated.
32 devices in a mesh: fs: 8 (over z, x), tp: 4 (over y, core).
Axes of the slice: x: 2, y: 2, z: 4, core: 2. Of those that a mesh axis runs over, the one named last changes fastest.
Arguments:
- tokens: bfloat16 [6144, 2048], P('fs', 'tp'), may hold values from -6 to 6
- ffn_one_gain: float32 [2048], replicated, may hold values from 0.1 to 1.9
- ffn_one_gate: bfloat16 [2048, 5632], P('fs', 'tp'), may hold values from -0.125 to 0.125
- ffn_one_up: bfloat16 [2048, 5632], P('fs', 'tp'), may hold values from -0.125 to 0.125
- ffn_one_down: bfloat16 [5632, 2048], P('tp', 'fs'), may hold values from -0.078125 to 0.078125
- mix_gain: float32 [2048], replicated, may hold values from 0.1 to 1.9
- conv_value: bfloat16 [2048, 1024], P('fs', 'tp'), may hold values from -0.125 to 0.125
- conv_gate: bfloat16 [2048, 1024], P('fs', 'tp'), may hold values from -0.125 to 0.125
- conv_kernel: float32 [31, 1024], P(None, 'tp'), may hold values from -15 to 15
- conv_ln_gain: float32 [1024], P('tp'), may hold values from 0.1 to 1.9
- conv_out: bfloat16 [1024, 2048], P('tp', 'fs'), may hold values from -0.1875 to 0.1875
- ffn_two_gain: float32 [2048], replicated, may hold values from 0.1 to 1.9
- ffn_two_gate: bfloat16 [2048, 5632], P('fs', 'tp'), may hold values from -0.125 to 0.125
- ffn_two_up: bfloat16 [2048, 5632], P('fs', 'tp'), may hold values from -0.125 to 0.125
- ffn_two_down: bfloat16 [5632, 2048], P('tp', 'fs'), may hold values from -0.078125 to 0.078125
Outputs:
- layer_out: bfloat16 [6144, 2048], P('fs', 'tp')
All inputs are finite; a program needn't handle non-finite values.
Results may differ from a plain program's by a relative error of at most 0.017.
Values may be sent and summed in bfloat16 or wider, within the bound.
A program may use at most 128 MiB of HBM per device.

v0:
```python
from functools import partial

import jax
import jax.numpy as jnp
from jax import lax
from jax.experimental import pallas as pl
from jax.experimental.pallas import tpu as pltpu
from jax.sharding import PartitionSpec as P

F32 = jnp.float32
BF16 = jnp.bfloat16
MESH = pl.DeviceIdType.MESH
NT = (((1,), (1,)), ((), ()))
PAD = 16


def split_fs(total):
    inner = 1
    while total % (inner * 2) == 0 and (inner * 2) ** 2 <= total:
        inner *= 2
    return total // inner, inner


class Plan:
    def __init__(self, fs, tp, tok, ws, cs, kernel_rows):
        self.fs, self.tp = fs, tp
        self.z, self.x = split_fs(fs)
        self.y = tp // 2
        self.rows, width = tok
        self.kb = ws[2]
        self.nb = width // self.kb
        self.ffh = ws[1] // 2
        self.ch = cs[0] // 3
        unit = 256 if self.ch % 256 == 0 else 128
        self.nw = unit
        self.ffp = -(-self.ffh // unit) * unit
        self.nc = self.ffp // unit
        self.lw = max(self.ffp, 3 * self.ch)
        self.half_rows = self.rows // 2
        self.cell = self.half_rows // self.y
        self.kw = kernel_rows
        self.dim = self.kb * fs


def body(g, *refs):
    (tok, ws, cs, gains, ck, cg, out) = refs[:7]
    (LW, XF, XR, ACC, HID, PP, RA, RB, RC, GB, SB, SR, AB) = refs[7:20]
    (s_loc, s_tok, zs, zr, xs, xr, ags, agr, as_, ar, bs, br, cs_s, cr, gys, gyr, gzs, gzr, gcs, gcr, sts, st_r, os_, orr) = refs[20:]
    Z, X, Y, TP, FS = g.z, g.x, g.y, g.tp, g.fs
    rows, kb, nb, ffh, ch = g.rows, g.kb, g.nb, g.ffh, g.ch
    TH, R = g.half_rows, g.cell
    fs_i, tp_i = lax.axis_index("fs"), lax.axis_index("tp")
    z, x = fs_i // X, fs_i % X
    y, core = tp_i // 2, tp_i % 2
    zp = z % 2
    oq = 1 - zp
    zb = z - zp
    zmate = zb + oq
    fs_mate = zmate * X + x
    tp_core = y * 2 + 1 - core

    def zx(j):
        if isinstance(j, int):
            hi, lo = j - j % 2, j % 2
        else:
            hi, lo = j - lax.rem(j, 2), lax.rem(j, 2)
        return xor2(zb, hi) + lo

    def xor2(a, b):
        r, bit = 0, 2
        while bit < Z:
            abit = lax.rem(a // bit, 2)
            bbit = (b // bit) % 2 if isinstance(b, int) else lax.rem(b // bit, 2)
            r = r + bit * lax.rem(abit + bbit, 2)
            bit *= 2
        return r

    def xor_z(k):
        r, bit = 0, 1
        while bit < Z:
            r = r + bit * lax.rem(lax.rem(z // bit, 2) + (k // bit) % 2, 2)
            bit *= 2
        return r

    def s_of(i):
        if isinstance(i, int):
            return zx(i // X) * X + lax.rem(x + i % X, X)
        return zx(i // X) * X + lax.rem(x + lax.rem(i, X), X)

    def rcopy(src, dst, ssem, rsem, fs_to, tp_to):
        return pltpu.make_async_remote_copy(
            src_ref=src, dst_ref=dst, send_sem=ssem, recv_sem=rsem,
            device_id=(fs_to, tp_to), device_id_type=MESH,
        )

    def yo(dy):
        return lax.rem(y + dy, Y)

    bar = pltpu.get_barrier_semaphore()
    peers = [(xor_z(k) * X + x, tp_i) for k in range(1, Z)]
    peers += [(z * X + lax.rem(x + dx, X), tp_i) for dx in range(1, X)]
    peers += [(fs_i, lax.rem(tp_i + dt, TP)) for dt in range(1, TP)]
    for f_to, t_to in peers:
        pl.semaphore_signal(bar, inc=1, device_id=(f_to, t_to), device_id_type=MESH)

    def local_weight(p):
        if p == 3:
            return pltpu.make_async_copy(cs, LW.at[3, fs_i, pl.ds(0, 3 * ch)], s_loc.at[p])
        src = ws.at[p if p < 3 else p - 1, pl.ds(pl.multiple_of(zp * ffh, 16), ffh)]
        return pltpu.make_async_copy(src, LW.at[p, fs_i, pl.ds(0, ffh)], s_loc.at[p])

    def local_tok(b):
        return pltpu.make_async_copy(
            tok.at[:, pl.ds(b * kb, kb)], XF.at[zp, tp_i * nb + b], s_tok.at[b]
        )

    for b in range(nb):
        local_tok(b).start()
    for p in range(7):
        local_weight(p).start()
    pl.semaphore_wait(bar, len(peers))

    def zsend(p, k):
        to = xor_z(k)
        if p == 3:
            src, dst = cs, LW.at[3, fs_i, pl.ds(0, 3 * ch)]
        else:
            src = ws.at[p if p < 3 else p - 1, pl.ds(pl.multiple_of(lax.rem(to, 2) * ffh, 16), ffh)]
            dst = LW.at[p, fs_i, pl.ds(0, ffh)]
        return rcopy(src, dst, zs.at[p, k], zr.at[p, k], to * X + x, tp_i)

    def xsend(p, j, dx):
        s = zx(j) * X + x
        ref = LW.at[p, s, pl.ds(0, 3 * ch if p == 3 else ffh)]
        return rcopy(ref, ref, xs.at[p, j, dx], xr.at[p, s], z * X + lax.rem(x + dx, X), tp_i)

    def xwait(p, s):
        ref = LW.at[p, s, pl.ds(0, 3 * ch if p == 3 else ffh)]
        rcopy(ref, ref, xs.at[p, 0, 1 % X], xr.at[p, s], z * X + x, tp_i).wait_recv()

    def start_zsend(m):
        p, k = m // (Z - 1), m % (Z - 1) + 1
        if p < 7:
            zsend(p, k).start()

    AHEAD = Z + 1

    def k_of(j):
        return jnp.where(zp == 0, j, j + 1 - 2 * (j % 2))

    def advance(n):
        if n >= 7 * Z:
            return
        p, j = n // Z, n % Z
        if j:
            start_zsend(p * (Z - 1) + j - 1 + AHEAD)

        if j < 2:
            @pl.when(zp == j)
            def _():
                local_weight(p).wait()

            @pl.when(zp != j)
            def _():
                zsend(p, 1).wait_recv()
        else:
            rcopy(LW.at[p, fs_i, pl.ds(0, 3 * ch if p == 3 else ffh)], LW.at[p, fs_i, pl.ds(0, 3 * ch if p == 3 else ffh)],
                  zs.at[p, 1], zr.at[p, k_of(j)], fs_i, tp_i).wait_recv()
        for dx in range(1, X):
            xsend(p, j, dx).start()

    def ag_piece(q, t):
        return XF.at[q, pl.ds(t * nb, nb)]

    def agz():
        r = ag_piece(zp, tp_i)
        return rcopy(r, r, ags.at[0], agr.at[0], fs_mate, tp_i)

    def agy(q, qi, dy):
        r = ag_piece(q, tp_i)
        return rcopy(r, r, ags.at[1 + qi * Y + dy], agr.at[1 + qi * Y + dy], fs_i, yo(dy) * 2 + core)

    def agy_wait(q, qi, dy):
        agy(q, qi, dy).wait_recv()

    def agc(q, qi, dy):
        r = ag_piece(q, lax.rem(y + Y - dy, Y) * 2 + core)
        n = 1 + 2 * Y + qi * Y + dy
        return rcopy(r, r, ags.at[n], agr.at[n], fs_i, tp_core)

    for b in range(nb):
        local_tok(b).wait()
    agz().start()
    for dy in range(1, Y):
        agy(zp, 0, dy).start()
    agc(zp, 0, 0).start()
    for m in range(AHEAD):
        start_zsend(m)
    if g.lw > ffh:
        def zero(i, c):
            for p in (0, 1, 2, 4, 5, 6):
                LW[p, i, ffh:] = jnp.zeros((g.lw - ffh, kb), BF16)
            return c
        lax.fori_loop(0, FS, zero, 0)
    GB[0:PAD] = jnp.zeros((PAD, ch), F32)
    GB[PAD + rows:] = jnp.zeros((PAD, ch), F32)
    advance(0)
    agz().wait_recv()
    for dy in range(1, Y):
        agy(oq, 1, dy).start()
    agc(oq, 1, 0).start()
    advance(1)
    for dy in range(1, Y):
        agy_wait(zp, 0, dy)
        agc(zp, 0, dy).start()
    advance(2)
    for dy in range(1, Y):
        agy_wait(oq, 1, dy)
        agc(oq, 1, dy).start()
    for n in range(3, Z):
        advance(n)
    for dy in range(Y):
        agc(zp, 0, dy).wait_recv()
        agc(oq, 1, dy).wait_recv()
    agz().wait_send()
    for dy in range(Y):
        agc(zp, 0, dy).wait_send()
        agc(oq, 1, dy).wait_send()
        if dy:
            agy(zp, 0, dy).wait_send()
            agy(oq, 1, dy).wait_send()

    my_cell = pl.multiple_of(core * TH + y * R, 16)

    def cell_of(yy):
        return pl.multiple_of(core * TH + yy * R, 16)

    def keep(s, c):
        XR[s] = XF[zp, s, pl.ds(my_cell, R)]
        return c

    lax.fori_loop(0, FS, keep, 0)

    NR = 64

    def normalize(q, layer):
        def chunk(c, carry):
            at = pl.ds(pl.multiple_of(c * NR, NR), NR)
            total = jnp.zeros((NR, kb), F32)
            for s in range(FS):
                v = XF[q, s, at].astype(F32)
                total = total + v * v
            scale = lax.rsqrt(jnp.sum(total, axis=1, keepdims=True) / g.dim + 1e-06)
            for s in range(FS):
                XF[q, s, at] = (XF[q, s, at].astype(F32) * scale * gains[layer, s]).astype(BF16)
            return carry
        lax.fori_loop(0, rows // NR, chunk, 0)

    def up_piece(p, half, j):
        def each(e, c):
            s = zx(j) * X + lax.rem(x + e, X)

            @pl.when(e > 0)
            def _():
                xwait(p, s)

            def seq(t, c2):
                q, n = t // g.nc, lax.rem(t, g.nc)
                w = LW[p, s, pl.ds(pl.multiple_of(n * g.nw, g.nw), g.nw)]
                d = lax.dot_general(XF[q, s], w, NT, preferred_element_type=F32)
                if j == 0:
                    @pl.when(e == 0)
                    def _():
                        ACC[half, q, n] = d

                    @pl.when(e > 0)
                    def _():
                        ACC[half, q, n] += d
                else:
                    ACC[half, q, n] += d
                return c2
            lax.fori_loop(0, 2 * g.nc, seq, 0)
            return c
        lax.fori_loop(0, X, each, 0)

    def a_copy(s, nq):
        at = pl.ds(pl.multiple_of((1 - core) * TH, 16), TH)
        here = pl.ds(0, TH)
        return rcopy(PP.at[s, pl.ds(0, nq), at], RA.at[s, pl.ds(0, nq), here], as_.at[s], ar.at[s], fs_i, tp_core)

    def b_copy(s, nq, dy):
        return rcopy(PP.at[s, pl.ds(0, nq), pl.ds(cell_of(yo(dy)), R)], RB.at[dy - 1, s, pl.ds(0, nq)],
                     bs.at[s, dy], br.at[s, dy], fs_i, yo(dy) * 2 + core)

    def c_copy(s):
        return rcopy(PP.at[s, oq, pl.ds(my_cell, R)], RC.at[s], cs_s.at[s], cr.at[s], fs_mate, tp_i)

    def stage_b(s, nq):
        a_copy(s, nq).wait_recv()
        mine = pl.ds(pl.multiple_of(core * TH, 16), TH)
        for q in range(nq):
            PP[s, q, mine] = (PP[s, q, mine].astype(F32) + RA[s, q].astype(F32)).astype(BF16)
        for dy in range(1, Y):
            b_copy(s, nq, dy).start()

    def b_sum(s, q):
        total = PP[s, q, pl.ds(my_cell, R)].astype(F32)
        for dy in range(1, Y):
            total = total + RB[dy - 1, s, q].astype(F32)
        return total

    def stage_c(s):
        for dy in range(1, Y):
            b_copy(s, 2, dy).wait_recv()
        PP[s, oq, pl.ds(my_cell, R)] = b_sum(s, oq).astype(BF16)
        c_copy(s).start()

    def ffn_sum(s):
        c_copy(s).wait_recv()
        total = b_sum(s, zp) + RC[s].astype(F32)
        return (XR[s].astype(F32) + 0.5 * total).astype(BF16)

    def gy_copy(q, qi, s, dy, yy):
        r = XF.at[q, s, pl.ds(cell_of(yy), R)]
        return rcopy(r, r, gys.at[qi, s, dy], gyr.at[qi, s, dy], fs_i, yo(dy) * 2 + core)

    def gz_copy(s):
        r = XF.at[zp, s, pl.ds(my_cell, R)]
        return rcopy(r, r, gzs.at[s], gzr.at[s], fs_mate, tp_i)

    def gc_copy(q, qi):
        r = XF.at[q, :, pl.ds(pl.multiple_of(core * TH, 16), TH)]
        return rcopy(r, r, gcs.at[qi], gcr.at[qi], fs_i, tp_core)

    def loop(n, f):
        def step(i, c):
            f(i)
            return c
        lax.fori_loop(0, n, step, 0)

    def half_step(p0, n0, finish, fill):
        n = n0
        for half in range(2):
            for j in range(Z):
                while n < (p0 + half) * Z + j + 2:
                    advance(n)
                    n += 1
                up_piece(p0 + half, half, j)

        def act(t):
            q = t // (rows // NR)
            at = pl.ds(pl.multiple_of(lax.rem(t, rows // NR) * NR, NR), NR)
            for c in range(g.nc):
                gate = ACC[0, q, c, at]
                HID[q, at, c * g.nw:(c + 1) * g.nw] = (gate * jax.nn.sigmoid(gate) * ACC[1, q, c, at]).astype(BF16)
        loop(2 * (rows // NR), act)

        for j in range(Z):
            while n < (p0 + 2) * Z + j + 2:
                advance(n)
                n += 1

            def each(e):
                i = j * X + e
                s = s_of(i)

                @pl.when(e > 0)
                def _():
                    xwait(p0 + 2, s)

                def seq(q):
                    PP[s, q] = jnp.dot(HID[q], LW[p0 + 2, s, pl.ds(0, g.ffp)], preferred_element_type=F32).astype(BF16)
                loop(2, seq)
                a_copy(s, 2).start()

                @pl.when(i >= 1)
                def _():
                    stage_b(s_of(i - 1), 2)

                @pl.when(i >= 2)
                def _():
                    stage_c(s_of(i - 2))

                @pl.when(i >= 3)
                def _():
                    finish(s_of(i - 3))
            loop(X, each)
        stage_b(s_of(FS - 1), 2)
        stage_c(s_of(FS - 2))
        finish(s_of(FS - 3))
        fill(n)
        stage_c(s_of(FS - 1))
        finish(s_of(FS - 2))
        finish(s_of(FS - 1))

    def sends_done(s):
        a_copy(s, 2).wait_send()
        c_copy(s).wait_send()
        for dy in range(1, Y):
            b_copy(s, 2, dy).wait_send()

    normalize(0, 0)
    normalize(1, 0)

    def finish_one(s):
        v = ffn_sum(s)
        XR[s] = v
        XF[zp, s, pl.ds(my_cell, R)] = v
        for dy in range(1, Y):
            gy_copy(zp, 0, s, dy, y).start()

    def fill_one(n):
        for k in range(n, 4 * Z):
            advance(k)

    half_step(0, Z, finish_one, fill_one)
    n = 4 * Z

    def own_arrived(s):
        for dy in range(1, Y):
            gy_copy(zp, 0, s, dy, y).wait_recv()
    loop(FS, own_arrived)
    gc_copy(zp, 0).start()
    loop(FS, sends_done)

    def own_sent(s):
        for dy in range(1, Y):
            gy_copy(zp, 0, s, dy, y).wait_send()
    loop(FS, own_sent)
    gc_copy(zp, 0).wait()

    normalize(zp, 1)

    def mix(i):
        e = lax.rem(i, X)
        s = s_of(i)

        @pl.when(e > 0)
        def _():
            xwait(3, s)
        for part in range(2):
            d = lax.dot_general(XF[zp, s], LW[3, s, part * ch:(part + 1) * ch], NT, preferred_element_type=F32)

            @pl.when(i == 0)
            def _():
                ACC[part, 0, 0] = d

            @pl.when(i > 0)
            def _():
                ACC[part, 0, 0] += d
    loop(FS, mix)

    def gated(t):
        at = pl.multiple_of(t * NR, NR)
        gate = ACC[1, 0, 0, pl.ds(at, NR)]
        GB[pl.ds(pl.multiple_of(at + PAD, 16), NR)] = ACC[0, 0, 0, pl.ds(at, NR)] * jax.nn.sigmoid(gate)
    loop(rows // NR, gated)

    off = PAD - g.kw // 2
    lanes = 128

    def taps(t):
        at = pl.multiple_of(t * NR, NR)
        sum_one = jnp.zeros((NR, 1), F32)
        sum_two = jnp.zeros((NR, 1), F32)
        for c in range(ch // lanes):
            cols = slice(c * lanes, (c + 1) * lanes)
            window = GB[pl.ds(at, NR + 2 * PAD), cols]
            total = jnp.zeros((NR, lanes), F32)
            for k in range(g.kw):
                total = total + ck[k:k + 1, cols] * window[k + off:k + off + NR]
            ACC[0, 1, 0, pl.ds(at, NR), cols] = total
            sum_one = sum_one + jnp.sum(total, axis=1, keepdims=True)
            sum_two = sum_two + jnp.sum(total * total, axis=1, keepdims=True)
        which = lax.broadcasted_iota(jnp.int32, (NR, 128), 1)
        AB[pl.ds(at, NR)] = jnp.where(which == 0, sum_one, jnp.where(which == 1, sum_two, 0.0))
    loop(rows // NR, taps)

    def flip(t):
        at = pl.ds(pl.multiple_of(t * 128, 128), 128)
        SB[:, at] = AB[at].T[0:8]
    loop(rows // 128, flip)

    def st_copy(dt):
        return rcopy(SB, SR.at[dt - 1], sts.at[dt], st_r.at[dt], fs_i, lax.rem(tp_i + dt, TP))

    for dt in range(1, TP):
        st_copy(dt).start()
    advance(n)
    n += 1
    for dt in range(1, TP):
        st_copy(dt).wait()

    def unflip(t):
        at = pl.ds(pl.multiple_of(t * 128, 128), 128)
        total = SB[:, at]
        for dt in range(1, TP):
            total = total + SR[dt - 1, :, at]
        AB[at] = jnp.concatenate([total, jnp.zeros((120, 128), F32)], axis=0).T
    loop(rows // 128, unflip)

    def activate(t):
        at = pl.ds(pl.multiple_of(t * NR, NR), NR)
        stats = AB[at]
        mean = stats[:, 0:1] / (ch * TP)
        var = stats[:, 1:2] / (ch * TP) - mean * mean
        v = (ACC[0, 1, 0, at] - mean) * lax.rsqrt(var + 1e-05) * cg[...]
        HID[0, at, 0:ch] = (v * jax.nn.sigmoid(v)).astype(BF16)
    loop(rows // NR, activate)

    def mixed(s):
        b_total = b_sum(s, 0)
        v = (XR[s].astype(F32) + b_total).astype(BF16)
        XR[s] = v
        XF[zp, s, pl.ds(my_cell, R)] = v
        gz_copy(s).start()
        for dy in range(1, Y):
            gy_copy(zp, 0, s, dy, y).start()

    def mixed_block(s):
        for dy in range(1, Y):
            b_copy(s, 1, dy).wait_recv()
        mixed(s)

    def pass_on(s):
        gz_copy(s).wait_recv()
        for dy in range(1, Y):
            gy_copy(oq, 1, s, dy, y).start()

    def project(i):
        s = s_of(i)
        PP[s, 0] = jnp.dot(HID[0, :, 0:ch], LW[3, s, 2 * ch:3 * ch], preferred_element_type=F32).astype(BF16)
        a_copy(s, 1).start()

        @pl.when(i >= 1)
        def _():
            stage_b(s_of(i - 1), 1)
    loop(FS, project)
    stage_b(s_of(FS - 1), 1)
    for i in range(FS + 2):
        if i < FS:
            mixed_block(s_of(i))
        if i >= 2:
            pass_on(s_of(i - 2))
        if i % 2 == 1 and n < 6 * Z:
            advance(n)
            n += 1

    def all_arrived(s):
        for dy in range(1, Y):
            gy_copy(zp, 0, s, dy, y).wait_recv()
    loop(FS, all_arrived)
    gc_copy(zp, 0).start()

    def rest_arrived(s):
        for dy in range(1, Y):
            gy_copy(oq, 1, s, dy, y).wait_recv()
    loop(FS, rest_arrived)
    gc_copy(oq, 1).start()

    def mix_sends(s):
        a_copy(s, 1).wait_send()
        gz_copy(s).wait_send()
        for dy in range(1, Y):
            b_copy(s, 1, dy).wait_send()
            gy_copy(zp, 0, s, dy, y).wait_send()
            gy_copy(oq, 1, s, dy, y).wait_send()
    loop(FS, mix_sends)
    gc_copy(zp, 0).wait()
    gc_copy(oq, 1).wait()

    normalize(0, 2)
    normalize(1, 2)

    def o_copy(s, slot):
        owner = s // nb
        b = lax.rem(s, nb)
        return rcopy(XR.at[s], out.at[b, pl.ds(my_cell, R)], os_.at[s], orr.at[b, slot], fs_i, owner)

    def finish_two(s):
        v = ffn_sum(s)
        owner = s // nb
        XR[s] = v

        @pl.when(owner == tp_i)
        def _():
            out[lax.rem(s, nb), pl.ds(my_cell, R)] = v

        @pl.when(owner != tp_i)
        def _():
            o_copy(s, lax.rem(tp_i - owner + TP, TP)).start()

    def fill_two(n):
        pass

    half_step(4, n, finish_two, fill_two)

    for b in range(nb):
        for slot in range(1, TP):
            rcopy(XR.at[0], out.at[b, pl.ds(0, R)], os_.at[0], orr.at[b, slot], fs_i, tp_i).wait_recv()

    def out_sent(s):
        @pl.when(s // nb != tp_i)
        def _():
            o_copy(s, 0).wait_send()
    loop(FS, out_sent)
    loop(FS, sends_done)
    for p in range(7):
        for k in range(1, Z):
            zsend(p, k).wait_send()
        for j in range(Z):
            for dx in range(1, X):
                xsend(p, j, dx).wait_send()


def per_device(fs, tp, tokens, g0, wg0, wu0, wd0, g1, cv, cgate, ck, cln, co, g2, wg1, wu1, wd1):
    ws = jnp.stack([wg0.T, wu0.T, wd0, wg1.T, wu1.T, wd1])
    cs = jnp.concatenate([cv.T, cgate.T, co], axis=0)
    g = Plan(fs, tp, tokens.shape, ws.shape, cs.shape, ck.shape[0])
    gains = jnp.stack([g0, g1, g2]).reshape(3, fs, 1, g.kb)
    Z, X, Y, TP, FS = g.z, g.x, g.y, g.tp, g.fs
    dma = pltpu.SemaphoreType.DMA
    vm = pltpu.VMEM
    scratch = [
        vm((7, FS, g.lw, g.kb), BF16),
        vm((2, FS, g.rows, g.kb), BF16),
        vm((FS, g.cell, g.kb), BF16),
        vm((2, 2, g.nc, g.rows, g.nw), F32),
        vm((2, g.rows, g.ffp), BF16),
        vm((FS, 2, g.rows, g.kb), BF16),
        vm((FS, 2, g.half_rows, g.kb), BF16),
        vm((Y - 1, FS, 2, g.cell, g.kb), BF16),
        vm((FS, g.cell, g.kb), BF16),
        vm((g.rows + 2 * PAD, g.ch), F32),
        vm((8, g.rows), F32),
        vm((TP - 1, 8, g.rows), F32),
        vm((g.rows, 128), F32),
        dma((7,)), dma((g.nb,)),
        dma((7, Z)), dma((7, Z)),
        dma((7, Z, X)), dma((7, FS)),
        dma((1 + 4 * Y,)), dma((1 + 4 * Y,)),
        dma((FS,)), dma((FS,)),
        dma((FS, Y)), dma((FS, Y)),
        dma((FS,)), dma((FS,)),
        dma((2, FS, Y)), dma((2, FS, Y)),
        dma((FS,)), dma((FS,)),
        dma((2,)), dma((2,)),
        dma((TP,)), dma((TP,)),
        dma((FS,)), dma((g.nb, TP)),
    ]
    anyspace = pl.BlockSpec(memory_space=pl.ANY)
    vmem = pl.BlockSpec(memory_space=pltpu.VMEM)
    res = pl.pallas_call(
        partial(body, g),
        out_shape=jax.ShapeDtypeStruct((g.nb, g.rows, g.kb), BF16),
        in_specs=[anyspace, anyspace, anyspace, vmem, vmem, vmem],
        out_specs=vmem,
        scratch_shapes=scratch,
        compiler_params=pltpu.CompilerParams(
            collective_id=0, has_side_effects=True, vmem_limit_bytes=67043328
        ),
        name="layer",
    )(tokens, ws, cs, gains, ck, cln.reshape(1, -1))
    return res.transpose(1, 0, 2).reshape(g.rows, g.nb * g.kb)


def solution(mesh):
    fs, tp = mesh.shape["fs"], mesh.shape["tp"]
    both = P("fs", "tp")
    down = P("tp", "fs")
    in_specs = (both, P(), both, both, down, P(), both, both, P(None, "tp"), P("tp"), down, P(), both, both, down)
    return jax.shard_map(
        partial(per_device, fs, tp), mesh=mesh, in_specs=in_specs, out_specs=both, check_vma=False
    )
```

profile of v0, /device:TPU:27, one launch (start us, length us, event | category | flops | bytes accessed | tf_op | source)
XLA Modules:
  0.0 400.8 jit_solution(1363415379466406879)
XLA Ops:
  0.0 0.0 copy-start
  0.0 0.0 copy-start.1
  0.0 1.5 copy.22
  1.5 0.0 copy-start.2
  1.5 0.9 bitcast_dynamic-update-slice_fusion.3
  2.4 1.4 copy.23
  3.8 0.9 bitcast_dynamic-update-slice_fusion.2
  4.7 0.0 copy-done
  4.7 0.0 copy-start.4
  4.7 0.0 copy-start.5
  4.7 0.0 copy-start.6
  4.7 0.9 bitcast_dynamic-update-slice_fusion.5
  5.7 0.0 copy-done.1
  5.7 0.0 copy-start.3
  5.7 0.0 copy-start.7
  5.7 0.0 copy-start.8
  5.7 0.0 copy-start.9
  5.7 0.3 copy.24
  6.0 0.9 bitcast_dynamic-update-slice_fusion.1
  6.9 0.0 copy-done.2
  6.9 0.3 copy.25
  7.2 0.9 bitcast_dynamic-update-slice_fusion
  8.1 0.0 copy-done.3
  8.1 0.9 bitcast_dynamic-update-slice_fusion.4.refs_1_
  9.0 0.0 copy-done.4
  9.0 0.1 copy.26
  9.1 0.0 copy-done.5
  9.1 0.1 copy.27
  9.2 0.0 copy-done.6
  9.2 0.8 pad_maximum_fusion.refs_2_
  10.0 0.0 copy-done.7
  10.0 0.0 copy-done.8
  10.0 0.0 copy-done.9
  10.0 0.6 pad_maximum_fusion.1.refs_3_
  10.6 387.6 %layer.1 = bf16[2,768,256]{2,1,0:T(8,128)(2,1)} custom-call(bf16[768,512]{1,0:T(8,128)(2,1)} %refs_0_.1, bf16[6,1408,256]{2,1,0:T(8,128)(2,1)} %bitcast_dynamic-update-slice_fusion.4.refs_1_, bf16[768,256]{1,0:T(8,128)(2,1)} %pad_maximum_fusion.refs_2_, f32[3,8,1,256]{3,2,1,0:T(1,128)} %pad_maximum_fusion.1.refs_3_, f32[31,256]{1,0:T(8,128)} %refs_4_.1, ...), custom_call_target="tpu_custom_call" | custom-call | tf_op jit(solution)/shard_map/layer/pallas_call | solution.py:653
  398.3 1.4 copy.28
  399.7 1.2 copy.29
Async XLA Ops:
  0.0 4.7 %copy-start = (bf16[1408,256]{1,0:T(8,128)(2,1)S(1)}, bf16[1408,256]{1,0:T(8,128)(2,1)}, u32[]{:S(2)}) copy-start(bf16[1408,256]{1,0:T(8,128)(2,1)} %param.19) | copy-start | bytes 2162692
  0.0 5.7 %copy-start.1 = (bf16[256,1408]{1,0:T(8,128)(2,1)S(1)}, bf16[256,1408]{1,0:T(8,128)(2,1)}, u32[]{:S(2)}) copy-start(bf16[256,1408]{1,0:T(8,128)(2,1)} %param.27) | copy-start | bytes 2162692
  1.5 5.4 %copy-start.2 = (bf16[256,1408]{1,0:T(8,128)(2,1)S(1)}, bf16[256,1408]{1,0:T(8,128)(2,1)}, u32[]{:S(2)}) copy-start(bf16[256,1408]{1,0:T(8,128)(2,1)} %param.28) | copy-start | bytes 2162692
  4.7 4.2 %copy-start.4 = (bf16[256,256]{1,0:T(8,128)(2,1)S(1)}, bf16[256,256]{1,0:T(8,128)(2,1)}, u32[]{:S(2)}) copy-start(bf16[256,256]{1,0:T(8,128)(2,1)} %param.21) | copy-start | bytes 393220
  4.7 4.3 %copy-start.5 = (bf16[256,256]{1,0:T(8,128)(2,1)S(1)}, bf16[256,256]{1,0:T(8,128)(2,1)}, u32[]{:S(2)}) copy-start(bf16[256,256]{1,0:T(8,128)(2,1)} %param.22) | copy-start | bytes 393220
  4.7 4.5 %copy-start.6 = (bf16[256,256]{1,0:T(8,128)(2,1)S(1)}, bf16[256,256]{1,0:T(8,128)(2,1)}, u32[]{:S(2)}) copy-start(bf16[256,256]{1,0:T(8,128)(2,1)} %param.25) | copy-start | bytes 393220
  5.7 2.4 copy-start.3
  5.7 4.3 %copy-start.7 = (f32[2048]{0:T(1024)S(1)}, f32[2048]{0:T(1024)}, u32[]{:S(2)}) copy-start(f32[2048]{0:T(1024)} %param.26) | copy-start | bytes 24580
  5.7 4.3 %copy-start.8 = (f32[2048]{0:T(1024)S(1)}, f32[2048]{0:T(1024)}, u32[]{:S(2)}) copy-start(f32[2048]{0:T(1024)} %param.20) | copy-start | bytes 24580
  5.7 4.3 %copy-start.9 = (f32[2048]{0:T(1024)S(1)}, f32[2048]{0:T(1024)}, u32[]{:S(2)}) copy-start(f32[2048]{0:T(1024)} %param.16) | copy-start | bytes 24580
where the time goes:
time: 401 us
  Pallas kernels  388 us (97%)
  local copies, waits for them, and re-layouts  11.7 us (3%)
    pallas_call x1, Pallas kernels, per_device(): pl.pallas_call(partial(body, g), out_shape=jax.ShapeDtypeStruct((g.nb, g....  388 us
    unnamed x31, local copies, waits for them, and re-layouts  8.22 us

commit v1 on v0

v1 whole, which is shorter than its diff:
```python
from functools import partial

import jax
import jax.numpy as jnp
from jax import lax
from jax.experimental import pallas as pl
from jax.experimental.pallas import tpu as pltpu
from jax.sharding import PartitionSpec as P

F32 = jnp.float32
BF16 = jnp.bfloat16
MESH = pl.DeviceIdType.MESH
NT = (((1,), (1,)), ((), ()))
PAD = 16


def split_fs(total):
    inner = 1
    while total % (inner * 2) == 0 and (inner * 2) ** 2 <= total:
        inner *= 2
    return total // inner, inner


class Plan:
    def __init__(self, fs, tp, tok, ws, co, kernel_rows):
        self.fs, self.tp = fs, tp
        self.z, self.x = split_fs(fs)
        self.y = tp // 2
        self.rows, width = tok
        self.kb = ws[1]
        self.nb = width // self.kb
        self.ffh = ws[0] // 2
        self.ch = co[0]
        unit = 256 if self.ch % 256 == 0 else 128
        self.ffp = -(-self.ffh // unit) * unit
        self.lw = max(self.ffp, 3 * self.ch)
        self.half_rows = self.rows // 2
        self.cell = self.half_rows // self.y
        self.kw = kernel_rows
        self.dim = self.kb * fs


class Marks:
    def __init__(self):
        self.open = None

    def __call__(self, name):
        if self.open is not None:
            self.open.__exit__(None, None, None)
        self.open = None
        if name is not None:
            self.open = jax.named_scope(name)
            self.open.__enter__()


def body(g, *refs):
    mark = Marks()
    mark("entry")
    (tok, *ws, cv, cgate, co, ga, gb, gc, ck, cg, out) = refs[:16]
    (LW, XF, XR, ACC, HID, PP, RA, RB, RC, RD, RE, RF, GB, CV, SB, SR, AB) = refs[16:33]
    gains = (ga, gb, gc)
    (s_loc, s_conv, s_tok, zs, zr, xs, xr, ags, agr, as_, ar, bs, br, cs_s, cr, ds, dr, es, er, fss, fr, gys, gyr, gzs, gzr, gcs, gcr, sts, st_r, os_, orr) = refs[33:]
    Z, X, Y, TP, FS = g.z, g.x, g.y, g.tp, g.fs
    rows, kb, nb, ffh, ch = g.rows, g.kb, g.nb, g.ffh, g.ch
    TH, R = g.half_rows, g.cell
    fs_i, tp_i = lax.axis_index("fs"), lax.axis_index("tp")
    z, x = fs_i // X, fs_i % X
    y, core = tp_i // 2, tp_i % 2
    zp = z % 2
    oq = 1 - zp
    zb = z - zp
    zmate = zb + oq
    fs_mate = zmate * X + x
    tp_core = y * 2 + 1 - core

    def zx(j):
        if isinstance(j, int):
            hi, lo = j - j % 2, j % 2
        else:
            hi, lo = j - lax.rem(j, 2), lax.rem(j, 2)
        return xor2(zb, hi) + lo

    def xor2(a, b):
        r, bit = 0, 2
        while bit < Z:
            abit = lax.rem(a // bit, 2)
            bbit = (b // bit) % 2 if isinstance(b, int) else lax.rem(b // bit, 2)
            r = r + bit * lax.rem(abit + bbit, 2)
            bit *= 2
        return r

    def xor_z(k):
        r, bit = 0, 1
        while bit < Z:
            r = r + bit * lax.rem(lax.rem(z // bit, 2) + (k // bit) % 2, 2)
            bit *= 2
        return r

    def s_of(i):
        if isinstance(i, int):
            return zx(i // X) * X + lax.rem(x + i % X, X)
        return zx(i // X) * X + lax.rem(x + lax.rem(i, X), X)

    def rcopy(src, dst, ssem, rsem, fs_to, tp_to):
        return pltpu.make_async_remote_copy(
            src_ref=src, dst_ref=dst, send_sem=ssem, recv_sem=rsem,
            device_id=(fs_to, tp_to), device_id_type=MESH,
        )

    def yo(dy):
        return lax.rem(y + dy, Y)

    bar = pltpu.get_barrier_semaphore()
    peers = [(xor_z(k) * X + x, tp_i) for k in range(1, Z)]
    peers += [(z * X + lax.rem(x + dx, X), tp_i) for dx in range(1, X)]
    peers += [(fs_i, lax.rem(tp_i + dt, TP)) for dt in range(1, TP)]
    for f_to, t_to in peers:
        pl.semaphore_signal(bar, inc=1, device_id=(f_to, t_to), device_id_type=MESH)

    def local_weight(p):
        if p == 3:
            return pltpu.make_async_copy(co, LW.at[3, fs_i, pl.ds(2 * ch, ch)], s_loc.at[p])
        src = ws[p if p < 3 else p - 1].at[pl.ds(pl.multiple_of(zp * ffh, 16), ffh)]
        return pltpu.make_async_copy(src, LW.at[p, fs_i, pl.ds(0, ffh)], s_loc.at[p])

    def local_tok(b):
        return pltpu.make_async_copy(
            tok.at[:, pl.ds(b * kb, kb)], XF.at[zp, tp_i * nb + b], s_tok.at[b]
        )

    for b in range(nb):
        local_tok(b).start()
    for p in range(7):
        local_weight(p).start()

    def local_conv(n):
        return pltpu.make_async_copy((cv, cgate)[n], HID.at[n, pl.ds(0, kb), pl.ds(0, ch)], s_conv.at[n])

    for n in range(2):
        local_conv(n).start()
    pl.semaphore_wait(bar, len(peers))

    def zsend(p, k):
        to = xor_z(k)
        if p == 3:
            src = dst = LW.at[3, fs_i, pl.ds(0, 3 * ch)]
        else:
            src = ws[p if p < 3 else p - 1].at[pl.ds(pl.multiple_of(lax.rem(to, 2) * ffh, 16), ffh)]
            dst = LW.at[p, fs_i, pl.ds(0, ffh)]
        return rcopy(src, dst, zs.at[p, k], zr.at[p, k], to * X + x, tp_i)

    def xsend(p, k, dx):
        s = (xor_z(k) if k else z) * X + x
        ref = LW.at[p, s, pl.ds(0, 3 * ch if p == 3 else ffh)]
        return rcopy(ref, ref, xs.at[p, k, dx], xr.at[p, s], z * X + lax.rem(x + dx, X), tp_i)

    def xwait(p, s):
        ref = LW.at[p, s, pl.ds(0, 3 * ch if p == 3 else ffh)]
        rcopy(ref, ref, xs.at[p, 0, 1 % X], xr.at[p, s], z * X + x, tp_i).wait_recv()

    inner = jnp.logical_and(z > 0, z < Z - 1)
    by_end = jnp.logical_or(z == 1, z == Z - 2)

    def relay(p):
        ref = LW.at[p, fs_mate, pl.ds(0, 3 * ch if p == 3 else ffh)]
        return rcopy(ref, ref, zs.at[p, 0], zr.at[p, Z - 1], xor_z(Z - 2) * X + x, tp_i)

    def near(p):
        zsend(p, 1).start()

    def near_two(p):
        @pl.when(jnp.logical_not(inner))
        def _():
            for k in range(2, Z - 1):
                zsend(p, k).start()

    def far(p, ks=tuple(range(2, Z))):
        @pl.when(inner)
        def _():
            for k in ks:
                zsend(p, k).start()

    hooks = {
        0: lambda: near(1),
        1: lambda: near_two(1),
        Z - 1: lambda: near(2),
        Z: lambda: near_two(2),
    }

    def own(p):
        if p < 7:
            if p != 3:
                local_weight(p).wait()
            for dx in range(1, X):
                xsend(p, 0, dx).start()

    done = [0]

    def advance(p, k):
        last = min(p, 6) * (Z - 1) + (k if p < 7 else Z - 1)
        while done[0] < last:
            m = done[0]
            q, d = m // (Z - 1), m % (Z - 1) + 1
            zsend(q, d).wait_recv()
            if d == 1:
                @pl.when(by_end)
                def _():
                    relay(q).start()
                if q < 6:
                    far(q + 1)
            if m in hooks:
                hooks[m]()
            for dx in range(1, X):
                xsend(q, d, dx).start()
            if m % (Z - 1) == Z - 2 and q >= 2:
                own(q + 1)
            done[0] = m + 1

    def ag_piece(q, t):
        return XF.at[q, pl.ds(t * nb, nb)]

    def agz():
        r = ag_piece(zp, tp_i)
        return rcopy(r, r, ags.at[0], agr.at[0], fs_mate, tp_i)

    def agy(q, qi, dy):
        r = ag_piece(q, tp_i)
        return rcopy(r, r, ags.at[1 + qi * Y + dy], agr.at[1 + qi * Y + dy], fs_i, yo(dy) * 2 + core)

    def agy_wait(q, qi, dy):
        agy(q, qi, dy).wait_recv()

    def agc(q, qi, dy):
        r = ag_piece(q, lax.rem(y + Y - dy, Y) * 2 + core)
        n = 1 + 2 * Y + qi * Y + dy
        return rcopy(r, r, ags.at[n], agr.at[n], fs_i, tp_core)

    mark("tok")
    for b in range(nb):
        local_tok(b).wait()
    agz().start()
    for dy in range(1, Y):
        agy(zp, 0, dy).start()
    agc(zp, 0, 0).start()
    near(0)
    near_two(0)
    far(0, tuple(range(3, Z)))
    for p in range(3):
        own(p)
    for n in range(2):
        local_conv(n).wait()
        LW[3, fs_i, n * ch:(n + 1) * ch] = HID[n, 0:kb, 0:ch].T
    local_weight(3).wait()
    if g.lw > ffh:
        def zero(i, c):
            for p in (0, 1, 2, 4, 5, 6):
                LW[p, i, ffh:] = jnp.zeros((g.lw - ffh, kb), BF16)
            return c
        lax.fori_loop(0, FS, zero, 0)
    GB[0:PAD] = jnp.zeros((PAD, ch), F32)
    GB[PAD + rows:] = jnp.zeros((PAD, ch), F32)
    mark("agz")
    agz().wait_recv()
    for dy in range(1, Y):
        agy(oq, 1, dy).start()
    agc(oq, 1, 0).start()
    far(0, (2,))
    mark("agy0")
    for dy in range(1, Y):
        agy_wait(zp, 0, dy)
        agc(zp, 0, dy).start()
    mark("adv01")
    advance(0, 1)
    mark("agy1")
    for dy in range(1, Y):
        agy_wait(oq, 1, dy)
        agc(oq, 1, dy).start()
    mark("adv03")
    advance(0, 2)
    mark("agc")
    for dy in range(Y):
        agc(zp, 0, dy).wait_recv()
        agc(oq, 1, dy).wait_recv()
    agz().wait_send()
    for dy in range(Y):
        agc(zp, 0, dy).wait_send()
        agc(oq, 1, dy).wait_send()
        if dy:
            agy(zp, 0, dy).wait_send()
            agy(oq, 1, dy).wait_send()

    my_cell = pl.multiple_of(core * TH + y * R, 16)

    def cell_of(yy):
        return pl.multiple_of(core * TH + yy * R, 16)

    mine = pl.ds(pl.multiple_of(core * TH, 16), TH)

    def keep(s, c):
        XR[s] = XF[zp, s, mine]
        return c

    lax.fori_loop(0, FS, keep, 0)

    NR = 64

    def normalize(q, layer):
        def chunk(c, carry):
            at = pl.ds(pl.multiple_of(c * NR, NR), NR)
            total = jnp.zeros((NR, kb), F32)
            for s in range(FS):
                v = XF[q, s, at].astype(F32)
                total = total + v * v
            scale = lax.rsqrt(jnp.sum(total, axis=1, keepdims=True) / g.dim + 1e-06)
            for s in range(FS):
                XF[q, s, at] = (XF[q, s, at].astype(F32) * scale * gains[layer][s]).astype(BF16)
            return carry
        lax.fori_loop(0, rows // NR, chunk, 0)

    MR = rows // 2

    def arrived(p):
        def one(i):
            @pl.when(lax.rem(i, X) > 0)
            def _():
                xwait(p, s_of(i))
        loop(FS, one)

    def features(p, q, at, width):
        total = None
        for s in range(FS):
            d = lax.dot_general(XF[q, s, at], LW[p, s, 0:width], NT, preferred_element_type=F32)
            total = d if total is None else total + d
        return total

    def chunks(n, f):
        def one(t):
            f(t // (rows // MR), pl.ds(pl.multiple_of(lax.rem(t, rows // MR) * MR, MR), MR))
        loop(n * (rows // MR), one)

    def loop(n, f):
        def step(i, c):
            f(i)
            return c
        lax.fori_loop(0, n, step, 0)

    def a_copy(s, nq):
        at = pl.ds(pl.multiple_of((1 - core) * TH, 16), TH)
        here = pl.ds(0, TH)
        return rcopy(PP.at[s, pl.ds(0, nq), at], RA.at[s, pl.ds(0, nq), here], as_.at[s], ar.at[s], fs_i, tp_core)

    def b_copy(s, dy):
        return rcopy(PP.at[s, :, pl.ds(cell_of(yo(dy)), R)], RB.at[dy - 1, s],
                     bs.at[s, dy], br.at[s, dy], fs_i, yo(dy) * 2 + core)

    def c_copy(s):
        return rcopy(PP.at[s, oq, pl.ds(my_cell, R)], RC.at[s], cs_s.at[s], cr.at[s], fs_mate, tp_i)

    def d_copy(s, dy):
        return rcopy(PP.at[s, 0, mine], RD.at[dy - 1, s], ds.at[s, dy], dr.at[s, dy], fs_i, yo(dy) * 2 + core)

    def stage_a(s, nq):
        a_copy(s, nq).wait_recv()
        for q in range(nq):
            PP[s, q, mine] = (PP[s, q, mine].astype(F32) + RA[s, q].astype(F32)).astype(BF16)

    def e_copy(s):
        return rcopy(PP.at[s, oq, mine], RE.at[s], es.at[s], er.at[s], fs_mate, tp_i)

    def f_copy(s, dy):
        return rcopy(PP.at[s, zp, pl.ds(cell_of(yo(dy)), R)], RF.at[dy - 1, s],
                     fss.at[s, dy], fr.at[s, dy], fs_i, yo(dy) * 2 + core)

    def by_parity(i, first, second):
        if isinstance(i, int):
            (second if i % 2 else first)()
        else:
            pl.when(lax.rem(i, 2) == 0)(first)
            pl.when(lax.rem(i, 2) == 1)(second)

    def stage_one(i):
        s = s_of(i)
        stage_a(s, 2)

        def even():
            for dy in range(1, Y):
                b_copy(s, dy).start()

        def odd():
            e_copy(s).start()
        by_parity(i, even, odd)

    def b_sum(s, q):
        total = PP[s, q, pl.ds(my_cell, R)].astype(F32)
        for dy in range(1, Y):
            total = total + RB[dy - 1, s, q].astype(F32)
        return total

    def stage_two(i):
        s = s_of(i)

        def even():
            for dy in range(1, Y):
                b_copy(s, dy).wait_recv()
            PP[s, oq, pl.ds(my_cell, R)] = b_sum(s, oq).astype(BF16)
            c_copy(s).start()

        def odd():
            e_copy(s).wait_recv()
            PP[s, zp, mine] = (PP[s, zp, mine].astype(F32) + RE[s].astype(F32)).astype(BF16)
            for dy in range(1, Y):
                f_copy(s, dy).start()
        by_parity(i, even, odd)

    def residual(s, total):
        return (XR[s, pl.ds(pl.multiple_of(y * R, 16), R)].astype(F32) + 0.5 * total).astype(BF16)

    def stage_three(i, put):
        s = s_of(i)

        def even():
            c_copy(s).wait_recv()
            put(s, residual(s, b_sum(s, zp) + RC[s].astype(F32)))

        def odd():
            total = PP[s, zp, pl.ds(my_cell, R)].astype(F32)
            for dy in range(1, Y):
                f_copy(s, dy).wait_recv()
                total = total + RF[dy - 1, s].astype(F32)
            put(s, residual(s, total))
        by_parity(i, even, odd)
        return s

    def sends_done(i):
        s = s_of(i)
        a_copy(s, 2).wait_send()

        def even():
            c_copy(s).wait_send()
            for dy in range(1, Y):
                b_copy(s, dy).wait_send()

        def odd():
            e_copy(s).wait_send()
            for dy in range(1, Y):
                f_copy(s, dy).wait_send()
        by_parity(i, even, odd)

    def gy_copy(q, qi, s, dy):
        r = XF.at[q, s, pl.ds(my_cell, R)]
        return rcopy(r, r, gys.at[s, dy], gyr.at[s, dy], fs_i, yo(dy) * 2 + core)

    def gc_copy(q, qi, s, dy, at):
        r = XF.at[q, s, at]
        return rcopy(r, r, gcs.at[qi, s, dy], gcr.at[qi, s, dy], fs_i, tp_core)

    def cell_from(dy):
        return pl.ds(cell_of(lax.rem(y - dy + Y, Y)), R)

    def plane_copy(s, at):
        r = XF.at[zp, s, at]
        return rcopy(r, r, gzs.at[s], gzr.at[s], fs_mate, tp_i)

    LAG_TWO, LAG_THREE = 3, 5

    def half_step(p0, before_down, plan, finish, after):
        mark(f"adv_p{p0}")
        advance(p0, Z - 1)
        advance(p0 + 1, 1)
        mark(f"wait_p{p0}")
        arrived(p0)
        mark(f"adv2_p{p0}")
        advance(p0 + 1, 2)
        mark(f"gate_p{p0}")

        def gate(q, at):
            ACC[q, at] = features(p0, q, at, g.ffp)
        chunks(2, gate)
        mark(f"adv_p{p0 + 1}")
        advance(p0 + 1, Z - 1)
        advance(p0 + 2, 1)
        mark(f"wait_p{p0 + 1}")
        arrived(p0 + 1)
        mark(f"up_p{p0 + 1}")

        def up(q, at):
            v = ACC[q, at]
            HID[q, at] = (v * jax.nn.sigmoid(v) * features(p0 + 1, q, at, g.ffp)).astype(BF16)
        chunks(2, up)

        before_down()
        for j in range(Z):
            mark(f"adv_p{p0 + 2}_{j}")
            plan[j]()

            def each(e):
                i = j * X + e
                s = s_of(i)

                @pl.when(e > 0)
                def _():
                    xwait(p0 + 2, s)

                def seq(q):
                    PP[s, q] = jnp.dot(HID[q], LW[p0 + 2, s, pl.ds(0, g.ffp)], preferred_element_type=F32).astype(BF16)
                loop(2, seq)
                a_copy(s, 2).start()

                @pl.when(i >= 1)
                def _():
                    stage_one(i - 1)

                @pl.when(i >= LAG_TWO)
                def _():
                    stage_two(i - LAG_TWO)

                @pl.when(i >= LAG_THREE)
                def _():
                    finish(i - LAG_THREE)
            mark(f"down_p{p0 + 2}_{j}")
            loop(X, each)
        mark("drain_a")
        stage_one(FS - 1)
        mark("drain_b")
        for i in range(FS - LAG_TWO, FS):
            stage_two(i)
            if i >= LAG_THREE - LAG_TWO:
                finish(i + LAG_TWO - LAG_THREE)
        mark("fill")
        after()
        mark("drain_c")
        for i in range(FS + LAG_TWO - LAG_THREE, FS):
            finish(i)

    mark("norm0")
    normalize(0, 0)
    normalize(1, 0)

    def put_one(s, v):
        XF[zp, s, pl.ds(my_cell, R)] = v

    def finish_one(i):
        s = stage_three(i, put_one)
        for dy in range(1, Y):
            gy_copy(zp, 0, s, dy).start()
        gc_copy(zp, 0, s, 0, pl.ds(my_cell, R)).start()

    def after_one():
        near(4)
        near_two(4)
        advance(3, Z - 1)

    half_step(
        0,
        lambda: near(3),
        [lambda: advance(2, 1), lambda: advance(2, 2), lambda: (near_two(3), advance(2, Z - 1)), lambda: advance(3, 1)],
        finish_one,
        after_one,
    )

    mark("own_arr")

    def from_y(s):
        for dy in range(1, Y):
            gy_copy(zp, 0, s, dy).wait_recv()
            gc_copy(zp, 0, s, dy, cell_from(dy)).start()
        XR[s] = XF[zp, s, mine]
    loop(FS, from_y)
    mark("own_core")
    near(5)
    loop(FS, sends_done)

    def one_sends(s):
        for dy in range(Y):
            if dy:
                gy_copy(zp, 0, s, dy).wait_send()
            gc_copy(zp, 0, s, dy, pl.ds(my_cell, R)).wait()
    loop(FS, one_sends)

    mark("adv41")
    advance(4, 1)
    mark("norm1")
    normalize(zp, 1)
    mark("mix")

    arrived(3)

    def mix(q, at):
        both = features(3, zp, at, 2 * ch)
        GB[pl.ds(pl.multiple_of(at.start + PAD, 16), MR)] = both[:, :ch] * jax.nn.sigmoid(both[:, ch:])
    chunks(1, mix)

    off = PAD - g.kw // 2
    lanes = 128

    def taps(t):
        at = pl.multiple_of(t * NR, NR)
        sum_one = jnp.zeros((NR, 1), F32)
        sum_two = jnp.zeros((NR, 1), F32)
        for c in range(ch // lanes):
            cols = slice(c * lanes, (c + 1) * lanes)
            window = GB[pl.ds(at, NR + 2 * PAD), cols]
            total = jnp.zeros((NR, lanes), F32)
            for r in range(8):
                taps_here = [k for k in range(g.kw) if (k + off) % 8 == r]
                shifted = window[r:max(taps_here) + off + NR]
                for k in taps_here:
                    total = total + ck[k:k + 1, cols] * shifted[k + off - r:k + off - r + NR]
            CV[pl.ds(at, NR), cols] = total
            sum_one = sum_one + jnp.sum(total, axis=1, keepdims=True)
            sum_two = sum_two + jnp.sum(total * total, axis=1, keepdims=True)
        which = lax.broadcasted_iota(jnp.int32, (NR, 128), 1)
        AB[pl.ds(at, NR)] = jnp.where(which == 0, sum_one, jnp.where(which == 1, sum_two, 0.0))
    mark("taps")
    loop(rows // NR, taps)
    mark("stats")

    def flip(t):
        at = pl.ds(pl.multiple_of(t * 128, 128), 128)
        SB[:, at] = AB[at].T[0:8]
    loop(rows // 128, flip)

    def st_copy(dt):
        return rcopy(SB, SR.at[dt - 1], sts.at[dt], st_r.at[dt], fs_i, lax.rem(tp_i + dt, TP))

    for dt in range(1, TP):
        st_copy(dt).start()
    near_two(5)
    advance(4, 2)
    for dt in range(1, TP):
        st_copy(dt).wait()

    def unflip(t):
        at = pl.ds(pl.multiple_of(t * 128, 128), 128)
        total = SB[:, at]
        for dt in range(1, TP):
            total = total + SR[dt - 1, :, at]
        AB[at] = jnp.concatenate([total, jnp.zeros((120, 128), F32)], axis=0).T
    loop(rows // 128, unflip)

    def activate(t):
        at = pl.ds(pl.multiple_of(t * NR, NR), NR)
        stats = AB[at]
        mean = stats[:, 0:1] / (ch * TP)
        var = stats[:, 1:2] / (ch * TP) - mean * mean
        v = (CV[at] - mean) * lax.rsqrt(var + 1e-05) * cg[...]
        HID[0, at, 0:ch] = (v * jax.nn.sigmoid(v)).astype(BF16)
    mark("active")
    loop(rows // NR, activate)

    def y_total(s):
        for dy in range(1, Y):
            d_copy(s, dy).wait_recv()
        own_part = PP[s, 0, mine].astype(F32)
        if Y == 2:
            return own_part + RD[0, s].astype(F32)
        total = jnp.zeros((TH, kb), F32)
        for yy in range(Y):
            slot = lax.rem(y - yy + Y, Y)
            term = RD[lax.max(slot - 1, 0), s].astype(F32)
            total = total + jnp.where(slot == 0, own_part, term)
        return total

    def mixed(i):
        s = s_of(i)
        v = (XR[s].astype(F32) + y_total(s)).astype(BF16)
        XR[s] = v
        XF[zp, s, mine] = v
        plane_copy(s, mine).start()
        gc_copy(zp, 0, s, 0, mine).start()

    def pass_on(i):
        s = s_of(i)
        plane_copy(s, mine).wait_recv()
        gc_copy(oq, 1, s, 0, mine).start()

    mark("project")

    def project(i):
        s = s_of(i)
        PP[s, 0] = jnp.dot(HID[0, :, 0:ch], LW[3, s, 2 * ch:3 * ch], preferred_element_type=F32).astype(BF16)
        a_copy(s, 1).start()

        @pl.when(i >= 1)
        def _():
            prev = s_of(i - 1)
            stage_a(prev, 1)
            for dy in range(1, Y):
                d_copy(prev, dy).start()
    loop(FS, project)
    last = s_of(FS - 1)
    stage_a(last, 1)
    for dy in range(1, Y):
        d_copy(last, dy).start()
    LAG_ON = 5
    for i in range(FS + LAG_ON):
        mark(f"mixed_{i}")
        if i < FS:
            mixed(i)
        if i == FS - 1:
            near(6)
            near_two(6)
        if i >= LAG_ON:
            pass_on(i - LAG_ON)
        if i % 2 == 1 and i < 2 * Z:
            mark(f"mixadv_{i}")
            advance(4 + (i // 2 + 2) // (Z - 1), (i // 2 + 2) % (Z - 1) + 1)
    mark("mixsends")

    def mix_sends(s):
        a_copy(s, 1).wait_send()
        plane_copy(s, mine).wait_send()
        gc_copy(zp, 0, s, 0, mine).wait()
        gc_copy(oq, 1, s, 0, mine).wait()
        for dy in range(1, Y):
            d_copy(s, dy).wait_send()
    loop(FS, mix_sends)

    mark("norm2")
    normalize(0, 2)
    normalize(1, 2)

    def o_copy(s, slot):
        owner = s // nb
        b = lax.rem(s, nb)
        return rcopy(XR.at[s, 0:R], out.at[pl.ds(my_cell, R), pl.ds(pl.multiple_of(b * kb, kb), kb)], os_.at[s], orr.at[b, slot], fs_i, owner)

    def put_two(s, v):
        XR[s, 0:R] = v

    def finish_two(i):
        s = stage_three(i, put_two)
        owner = s // nb

        @pl.when(owner == tp_i)
        def _():
            out[pl.ds(my_cell, R), pl.ds(pl.multiple_of(lax.rem(s, nb) * kb, kb), kb)] = XR[s, 0:R]

        @pl.when(owner != tp_i)
        def _():
            o_copy(s, lax.rem(tp_i - owner + TP, TP)).start()

    half_step(4, lambda: None, [partial(advance, 6, min(j + 1, Z - 1)) for j in range(Z)], finish_two, lambda: None)

    mark("out_wait")
    for b in range(nb):
        for slot in range(1, TP):
            rcopy(XR.at[0, 0:R], out.at[pl.ds(0, R), pl.ds(b * kb, kb)], os_.at[0], orr.at[b, slot], fs_i, tp_i).wait_recv()

    mark("end_sends")

    def out_sent(s):
        @pl.when(s // nb != tp_i)
        def _():
            o_copy(s, 0).wait_send()
    loop(FS, out_sent)

    loop(FS, sends_done)
    for p in range(7):
        for k in range(1, Z - 1):
            zsend(p, k).wait_send()

        @pl.when(inner)
        def _():
            zsend(p, Z - 1).wait_send()

        @pl.when(by_end)
        def _():
            relay(p).wait_send()
        for k in range(Z):
            for dx in range(1, X):
                xsend(p, k, dx).wait_send()
    mark(None)


def per_device(fs, tp, tokens, g0, wg0, wu0, wd0, g1, cv, cgate, ck, cln, co, g2, wg1, wu1, wd1):
    ws = [wg0.T, wu0.T, wd0, wg1.T, wu1.T, wd1]
    g = Plan(fs, tp, tokens.shape, wd0.shape, co.shape, ck.shape[0])
    gains = [v.reshape(fs, 1, g.kb) for v in (g0, g1, g2)]
    Z, X, Y, TP, FS = g.z, g.x, g.y, g.tp, g.fs
    dma = pltpu.SemaphoreType.DMA
    vm = pltpu.VMEM
    scratch = [
        vm((7, FS, g.lw, g.kb), BF16),
        vm((2, FS, g.rows, g.kb), BF16),
        vm((FS, g.half_rows, g.kb), BF16),
        vm((2, g.rows, g.ffp), F32),
        vm((2, g.rows, g.ffp), BF16),
        vm((FS, 2, g.rows, g.kb), BF16),
        vm((FS, 2, g.half_rows, g.kb), BF16),
        vm((Y - 1, FS, 2, g.cell, g.kb), BF16),
        vm((FS, g.cell, g.kb), BF16),
        vm((Y - 1, FS, g.half_rows, g.kb), BF16),
        vm((FS, g.half_rows, g.kb), BF16),
        vm((Y - 1, FS, g.cell, g.kb), BF16),
        vm((g.rows + 2 * PAD, g.ch), F32),
        vm((g.rows, g.ch), F32),
        vm((8, g.rows), F32),
        vm((TP - 1, 8, g.rows), F32),
        vm((g.rows, 128), F32),
        dma((7,)), dma((2,)), dma((g.nb,)),
        dma((7, Z)), dma((7, Z)),
        dma((7, Z, X)), dma((7, FS)),
        dma((1 + 4 * Y,)), dma((1 + 4 * Y,)),
        dma((FS,)), dma((FS,)),
        dma((FS, Y)), dma((FS, Y)),
        dma((FS,)), dma((FS,)),
        dma((FS, Y)), dma((FS, Y)),
        dma((FS,)), dma((FS,)),
        dma((FS, Y)), dma((FS, Y)),
        dma((FS, Y)), dma((FS, Y)),
        dma((FS,)), dma((FS,)),
        dma((2, FS, Y)), dma((2, FS, Y)),
        dma((TP,)), dma((TP,)),
        dma((FS,)), dma((g.nb, TP)),
    ]
    anyspace = pl.BlockSpec(memory_space=pl.ANY)
    vmem = pl.BlockSpec(memory_space=pltpu.VMEM)
    res = pl.pallas_call(
        partial(body, g),
        out_shape=jax.ShapeDtypeStruct((g.rows, g.nb * g.kb), BF16),
        in_specs=[anyspace] * 10 + [vmem] * 5,
        out_specs=vmem,
        scratch_shapes=scratch,
        compiler_params=pltpu.CompilerParams(
            collective_id=0, has_side_effects=True, vmem_limit_bytes=67043328
        ),
        name="layer",
    )(tokens, *ws, cv, cgate, co, *gains, ck, cln.reshape(1, -1))
    return res


def solution(mesh):
    fs, tp = mesh.shape["fs"], mesh.shape["tp"]
    both = P("fs", "tp")
    down = P("tp", "fs")
    in_specs = (both, P(), both, both, down, P(), both, both, P(None, "tp"), P("tp"), down, P(), both, both, down)
    return jax.shard_map(
        partial(per_device, fs, tp), mesh=mesh, in_specs=in_specs, out_specs=both, check_vma=False
    )
```

time: 401 us -> 328 us (0.82)
  Pallas kernels: 388 us -> 319 us
    pallas_call x1, Pallas kernels: 388 us -> 319 us  [per_device(): pl.pallas_call(partial(body, g), out_shape=jax.ShapeDtypeStruct((g.rows,...]
    unnamed x31 -> x11, local copies, waits for them, and re-layouts: 8.22 us -> 7.82 us
where the time goes in v1:
time: 328 us; the launch traced here: 327 us
  Pallas kernels  319 us (97%)
  local copies, waits for them, and re-layouts  7.82 us (2%)
    pallas_call x1, Pallas kernels, per_device(): pl.pallas_call(partial(body, g), out_shape=jax.ShapeDtypeStruct((g.rows,...  319 us
    unnamed x11, local copies, waits for them, and re-layouts  7.82 us

profile of v1, /device:TPU:27, one launch (start us, length us, event | category | flops | bytes accessed | tf_op | source)
XLA Modules:
  0.0 327.2 jit_solution(10413863255840515688)
XLA Ops:
  0.0 0.0 copy-start
  0.0 2.3 copy.16
  2.3 0.0 copy-done
  2.3 0.0 copy-start.1
  2.3 1.2 copy.17
  3.5 0.0 copy-done.1
  3.5 0.0 copy-start.2
  3.5 1.1 copy.18
  4.6 0.0 copy-done.2
  4.6 1.1 copy.19
  5.8 319.4 %layer.1 = bf16[768,512]{1,0:T(8,128)(2,1)} custom-call(bf16[768,512]{1,0:T(8,128)(2,1)} %refs_0_.1, bf16[1408,256]{1,0:T(8,128)(2,1)} %bitcast.8, bf16[1408,256]{1,0:T(8,128)(2,1)} %bitcast.9, bf16[1408,256]{1,0:T(8,128)(2,1)} %refs_3_.1, bf16[1408,256]{1,0:T(8,128)(2,1)} %bitcast.10, bf16[1408,256]{1,0:T(8,128)(2,1)} %bitcast.11, ...), custom_call_target="tpu_custom_call" | custom-call | tf_op jit(solution)/shard_map/layer/pallas_call | solution.py:819
  325.2 2.1 copy.21
Async XLA Ops:
  0.0 2.3 copy-start
  2.3 1.2 copy-start.1
  3.5 1.2 copy-start.2

commit v2 on v1

--- a/solution.py
+++ b/solution.py
@@ -165,6 +165,8 @@
         ref = LW.at[p, fs_mate, pl.ds(0, 3 * ch if p == 3 else ffh)]
         return rcopy(ref, ref, zs.at[p, 0], zr.at[p, Z - 1], xor_z(Z - 2) * X + x, tp_i)
 
+    MIDDLE = tuple(range(2, Z - 1))
+
     def near(p):
         zsend(p, 1).start()
 
@@ -174,7 +176,7 @@
             for k in range(2, Z - 1):
                 zsend(p, k).start()
 
-    def far(p, ks=tuple(range(2, Z))):
+    def far(p, ks):
         @pl.when(inner)
         def _():
             for k in ks:
@@ -206,8 +208,10 @@
                 @pl.when(by_end)
                 def _():
                     relay(q).start()
-                if q < 6:
-                    far(q + 1)
+                if q < 2:
+                    far(q + 1, MIDDLE)
+                if 1 <= q < 6:
+                    far(q + 1, (Z - 1,))
             if m in hooks:
                 hooks[m]()
             for dx in range(1, X):
@@ -244,7 +248,8 @@
     agc(zp, 0, 0).start()
     near(0)
     near_two(0)
-    far(0, tuple(range(3, Z)))
+    for p in range(2):
+        far(p, (Z - 1,))
     for p in range(3):
         own(p)
     for n in range(2):
@@ -264,7 +269,7 @@
     for dy in range(1, Y):
         agy(oq, 1, dy).start()
     agc(oq, 1, 0).start()
-    far(0, (2,))
+    far(0, MIDDLE)
     mark("agy0")
     for dy in range(1, Y):
         agy_wait(zp, 0, dy)
@@ -304,7 +309,7 @@
 
     NR = 64
 
-    def normalize(q, layer):
+    def normalize(q, layer, put=None):
         def chunk(c, carry):
             at = pl.ds(pl.multiple_of(c * NR, NR), NR)
             total = jnp.zeros((NR, kb), F32)
@@ -313,7 +318,11 @@
                 total = total + v * v
             scale = lax.rsqrt(jnp.sum(total, axis=1, keepdims=True) / g.dim + 1e-06)
             for s in range(FS):
-                XF[q, s, at] = (XF[q, s, at].astype(F32) * scale * gains[layer][s]).astype(BF16)
+                v = (XF[q, s, at].astype(F32) * scale * gains[layer][s]).astype(BF16)
+                if put is None:
+                    XF[q, s, at] = v
+                else:
+                    put(s, at, v)
             return carry
         lax.fori_loop(0, rows // NR, chunk, 0)
 
@@ -326,17 +335,18 @@
                 xwait(p, s_of(i))
         loop(FS, one)
 
-    def features(p, q, at, width):
+    def features(p, block, width):
         total = None
         for s in range(FS):
-            d = lax.dot_general(XF[q, s, at], LW[p, s, 0:width], NT, preferred_element_type=F32)
+            d = lax.dot_general(block(s), LW[p, s, 0:width], NT, preferred_element_type=F32)
             total = d if total is None else total + d
         return total
 
-    def chunks(n, f):
+    def chunks(qs, f):
         def one(t):
-            f(t // (rows // MR), pl.ds(pl.multiple_of(lax.rem(t, rows // MR) * MR, MR), MR))
-        loop(n * (rows // MR), one)
+            q = t // (rows // MR) if qs is None else qs
+            f(q, pl.ds(pl.multiple_of(lax.rem(t, rows // MR) * MR, MR), MR))
+        loop((2 if qs is None else 1) * (rows // MR), one)
 
     def loop(n, f):
         def step(i, c):
@@ -371,7 +381,12 @@
         return rcopy(PP.at[s, zp, pl.ds(cell_of(yo(dy)), R)], RF.at[dy - 1, s],
                      fss.at[s, dy], fr.at[s, dy], fs_i, yo(dy) * 2 + core)
 
+    turns = [False]
+
     def by_parity(i, first, second):
+        if not turns[0]:
+            first()
+            return
         if isinstance(i, int):
             (second if i % 2 else first)()
         else:
@@ -463,31 +478,18 @@
 
     LAG_TWO, LAG_THREE = 3, 5
 
-    def half_step(p0, before_down, plan, finish, after):
-        mark(f"adv_p{p0}")
-        advance(p0, Z - 1)
-        advance(p0 + 1, 1)
-        mark(f"wait_p{p0}")
-        arrived(p0)
-        mark(f"adv2_p{p0}")
-        advance(p0 + 1, 2)
-        mark(f"gate_p{p0}")
-
-        def gate(q, at):
-            ACC[q, at] = features(p0, q, at, g.ffp)
-        chunks(2, gate)
-        mark(f"adv_p{p0 + 1}")
-        advance(p0 + 1, Z - 1)
-        advance(p0 + 2, 1)
-        mark(f"wait_p{p0 + 1}")
-        arrived(p0 + 1)
-        mark(f"up_p{p0 + 1}")
-
-        def up(q, at):
+    def gate_rows(p0, block):
+        def f(q, at):
+            ACC[q, at] = features(p0, lambda s: block(q, s, at), g.ffp)
+        return f
+
+    def up_rows(p0, block):
+        def f(q, at):
             v = ACC[q, at]
-            HID[q, at] = (v * jax.nn.sigmoid(v) * features(p0 + 1, q, at, g.ffp)).astype(BF16)
-        chunks(2, up)
-
+            HID[q, at] = (v * jax.nn.sigmoid(v) * features(p0 + 1, lambda s: block(q, s, at), g.ffp)).astype(BF16)
+        return f
+
+    def down_and_sum(p0, before_down, plan, finish, before_last, after):
         before_down()
         for j in range(Z):
             mark(f"adv_p{p0 + 2}_{j}")
@@ -523,10 +525,13 @@
         stage_one(FS - 1)
         mark("drain_b")
         for i in range(FS - LAG_TWO, FS):
+            if i == FS - 1:
+                mark("fill")
+                before_last()
+                mark("drain_b2")
             stage_two(i)
             if i >= LAG_THREE - LAG_TWO:
                 finish(i + LAG_TWO - LAG_THREE)
-        mark("fill")
         after()
         mark("drain_c")
         for i in range(FS + LAG_TWO - LAG_THREE, FS):
@@ -545,17 +550,30 @@
             gy_copy(zp, 0, s, dy).start()
         gc_copy(zp, 0, s, 0, pl.ds(my_cell, R)).start()
 
-    def after_one():
-        near(4)
-        near_two(4)
-        advance(3, Z - 1)
-
-    half_step(
+    def from_xf(q, s, at):
+        return XF[q, s, at]
+
+    mark("adv_p0")
+    advance(1, 1)
+    mark("wait_p0")
+    arrived(0)
+    mark("adv2_p0")
+    advance(1, 2)
+    mark("gate_p0")
+    chunks(None, gate_rows(0, from_xf))
+    mark("adv_p1")
+    advance(2, 1)
+    mark("wait_p1")
+    arrived(1)
+    mark("up_p1")
+    chunks(None, up_rows(0, from_xf))
+    down_and_sum(
         0,
-        lambda: near(3),
+        lambda: (near(3), far(3, MIDDLE)),
         [lambda: advance(2, 1), lambda: advance(2, 2), lambda: (near_two(3), advance(2, Z - 1)), lambda: advance(3, 1)],
         finish_one,
-        after_one,
+        lambda: advance(3, Z - 1),
+        lambda: (near(4), near_two(4), far(4, MIDDLE), near(5), far(5, MIDDLE)),
     )
 
     mark("own_arr")
@@ -567,7 +585,7 @@
         XR[s] = XF[zp, s, mine]
     loop(FS, from_y)
     mark("own_core")
-    near(5)
+    near_two(5)
     loop(FS, sends_done)
 
     def one_sends(s):
@@ -577,8 +595,6 @@
             gc_copy(zp, 0, s, dy, pl.ds(my_cell, R)).wait()
     loop(FS, one_sends)
 
-    mark("adv41")
-    advance(4, 1)
     mark("norm1")
     normalize(zp, 1)
     mark("mix")
@@ -586,9 +602,9 @@
     arrived(3)
 
     def mix(q, at):
-        both = features(3, zp, at, 2 * ch)
+        both = features(3, lambda s: XF[zp, s, at], 2 * ch)
         GB[pl.ds(pl.multiple_of(at.start + PAD, 16), MR)] = both[:, :ch] * jax.nn.sigmoid(both[:, ch:])
-    chunks(1, mix)
+    chunks(zp, mix)
 
     off = PAD - g.kw // 2
     lanes = 128
@@ -625,8 +641,7 @@
 
     for dt in range(1, TP):
         st_copy(dt).start()
-    near_two(5)
-    advance(4, 2)
+    advance(4, 1)
     for dt in range(1, TP):
         st_copy(dt).wait()
 
@@ -666,59 +681,119 @@
         v = (XR[s].astype(F32) + y_total(s)).astype(BF16)
         XR[s] = v
         XF[zp, s, mine] = v
-        plane_copy(s, mine).start()
+        plane_copy(s, plane_rows(i)).start()
         gc_copy(zp, 0, s, 0, mine).start()
+
+    def whole(i):
+        return False
+
+    def plane_rows(i):
+        return mine if whole(i) else pl.ds(my_cell, R)
 
     def pass_on(i):
         s = s_of(i)
-        plane_copy(s, mine).wait_recv()
-        gc_copy(oq, 1, s, 0, mine).start()
-
-    mark("project")
+        plane_copy(s, plane_rows(i)).wait_recv()
+        gc_copy(oq, 1, s, 0, plane_rows(i)).start()
+        if not whole(i):
+            for dy in range(1, Y):
+                gy_copy(oq, 1, s, dy).start()
+
+    def last_hop(i):
+        if not whole(i):
+            s = s_of(i)
+            for dy in range(1, Y):
+                gy_copy(oq, 1, s, dy).wait_recv()
+                gc_copy(oq, 1, s, dy, cell_from(dy)).start()
+
+    def to_y(s):
+        stage_a(s, 1)
+        for dy in range(1, Y):
+            d_copy(s, dy).start()
 
     def project(i):
         s = s_of(i)
         PP[s, 0] = jnp.dot(HID[0, :, 0:ch], LW[3, s, 2 * ch:3 * ch], preferred_element_type=F32).astype(BF16)
         a_copy(s, 1).start()
 
-        @pl.when(i >= 1)
+        @pl.when(i >= 2)
         def _():
-            prev = s_of(i - 1)
-            stage_a(prev, 1)
-            for dy in range(1, Y):
-                d_copy(prev, dy).start()
+            to_y(s_of(i - 2))
     loop(FS, project)
-    last = s_of(FS - 1)
-    stage_a(last, 1)
-    for dy in range(1, Y):
-        d_copy(last, dy).start()
+    to_y(s_of(FS - 2))
+    to_y(s_of(FS - 1))
+    advance(4, 2)
     LAG_ON = 5
-    for i in range(FS + LAG_ON):
+    for i in range(FS):
         mark(f"mixed_{i}")
-        if i < FS:
-            mixed(i)
+        mixed(i)
+        if i == FS - 3:
+            near(6)
+            far(6, MIDDLE)
         if i == FS - 1:
-            near(6)
             near_two(6)
         if i >= LAG_ON:
             pass_on(i - LAG_ON)
         if i % 2 == 1 and i < 2 * Z:
             mark(f"mixadv_{i}")
             advance(4 + (i // 2 + 2) // (Z - 1), (i // 2 + 2) % (Z - 1) + 1)
+    mark("own2")
+
+    def own_ready(s):
+        gc_copy(zp, 0, s, 0, mine).wait_recv()
+    loop(FS, own_ready)
+
+    def put_own(s, at, v):
+        PP[s, 1, at] = v
+
+    def from_own(q, s, at):
+        return PP[s, 1, at]
+
+    mark("norm2")
+    normalize(zp, 2, put_own)
+    left = list(range(FS - LAG_ON, FS))
+    third = -(-len(left) // 3)
+    mark("pass_a")
+    for i in left[:third]:
+        pass_on(i)
+    mark("wait_p4")
+    arrived(4)
+    mark("gate_p4")
+    chunks(zp, gate_rows(4, from_own))
+    mark("pass_b")
+    for i in left[third:2 * third]:
+        pass_on(i)
+    mark("wait_p5")
+    arrived(5)
+    mark("up_p5")
+    chunks(zp, up_rows(4, from_own))
+    mark("pass_c")
+    for i in left[2 * third:]:
+        pass_on(i)
+    mark("adv61")
+    advance(6, 1)
     mark("mixsends")
 
-    def mix_sends(s):
+    for i in range(FS):
+        last_hop(i)
+    for i in range(FS):
+        s = s_of(i)
         a_copy(s, 1).wait_send()
-        plane_copy(s, mine).wait_send()
-        gc_copy(zp, 0, s, 0, mine).wait()
-        gc_copy(oq, 1, s, 0, mine).wait()
+        plane_copy(s, plane_rows(i)).wait_send()
+        gc_copy(zp, 0, s, 0, mine).wait_send()
+        gc_copy(oq, 1, s, 0, plane_rows(i)).wait()
         for dy in range(1, Y):
             d_copy(s, dy).wait_send()
-    loop(FS, mix_sends)
-
-    mark("norm2")
-    normalize(0, 2)
-    normalize(1, 2)
+            if not whole(i):
+                gy_copy(oq, 1, s, dy).wait_send()
+                gc_copy(oq, 1, s, dy, cell_from(dy)).wait()
+    mark("norm2b")
+    normalize(oq, 2)
+    mark("gate_p4b")
+    chunks(oq, gate_rows(4, from_xf))
+    mark("adv62")
+    advance(6, 2)
+    mark("up_p5b")
+    chunks(oq, up_rows(4, from_xf))
 
     def o_copy(s, slot):
         owner = s // nb
@@ -740,7 +815,8 @@
         def _():
             o_copy(s, lax.rem(tp_i - owner + TP, TP)).start()
 
-    half_step(4, lambda: None, [partial(advance, 6, min(j + 1, Z - 1)) for j in range(Z)], finish_two, lambda: None)
+    turns[0] = True
+    down_and_sum(4, lambda: None, [partial(advance, 6, Z - 1)] * Z, finish_two, lambda: None, lambda: None)
 
     mark("out_wait")
     for b in range(nb):

time: 328 us -> 301 us (0.918)
  Pallas kernels: 319 us -> 292 us
    pallas_call x1, Pallas kernels: 319 us -> 292 us  [per_device(): pl.pallas_call(partial(body, g), out_shape=jax.ShapeDtypeStruct((g.rows,...]
where the time goes in v2:
time: 301 us; the launch traced here: 300 us
  Pallas kernels  292 us (97%)
  local copies, waits for them, and re-layouts  7.82 us (3%)
    pallas_call x1, Pallas kernels, per_device(): pl.pallas_call(partial(body, g), out_shape=jax.ShapeDtypeStruct((g.rows,...  292 us
    unnamed x11, local copies, waits for them, and re-layouts  7.82 us

profile of v2, /device:TPU:27, one launch (start us, length us, event | category | flops | bytes accessed | tf_op | source)
XLA Modules:
  0.0 300.2 jit_solution(3684567285522380642)
XLA Ops:
  0.0 0.0 copy-start
  0.0 2.3 copy.16
  2.3 0.0 copy-done
  2.3 0.0 copy-start.1
  2.3 1.2 copy.17
  3.5 0.0 copy-done.1
  3.5 0.0 copy-start.2
  3.5 1.1 copy.18
  4.6 0.0 copy-done.2
  4.6 1.1 copy.19
  5.8 292.3 %layer.1 = bf16[768,512]{1,0:T(8,128)(2,1)} custom-call(bf16[768,512]{1,0:T(8,128)(2,1)} %refs_0_.1, bf16[1408,256]{1,0:T(8,128)(2,1)} %bitcast.8, bf16[1408,256]{1,0:T(8,128)(2,1)} %bitcast.9, bf16[1408,256]{1,0:T(8,128)(2,1)} %refs_3_.1, bf16[1408,256]{1,0:T(8,128)(2,1)} %bitcast.10, bf16[1408,256]{1,0:T(8,128)(2,1)} %bitcast.11, ...), custom_call_target="tpu_custom_call" | custom-call | tf_op jit(solution)/shard_map/layer/pallas_call | solution.py:895
  298.1 2.1 copy.21
Async XLA Ops:
  0.0 2.3 copy-start
  2.3 1.2 copy-start.1
  3.5 1.2 copy-start.2

commit v3 on v2

--- a/solution.py
+++ b/solution.py
@@ -37,6 +37,7 @@
         self.half_rows = self.rows // 2
         self.cell = self.half_rows // self.y
         self.kw = kernel_rows
+        self.turn = ws[0] % 128 == 0
         self.dim = self.kb * fs
 
 
@@ -57,9 +58,9 @@
     mark = Marks()
     mark("entry")
     (tok, *ws, cv, cgate, co, ga, gb, gc, ck, cg, out) = refs[:16]
-    (LW, XF, XR, ACC, HID, PP, RA, RB, RC, RD, RE, RF, GB, CV, SB, SR, AB) = refs[16:33]
+    (LW, XF, XR, ACC, HID, PP, RA, RB, RC, RD, RE, RF, GB, CV, SB, SR, AB, ST, TW) = refs[16:35]
     gains = (ga, gb, gc)
-    (s_loc, s_conv, s_tok, zs, zr, xs, xr, ags, agr, as_, ar, bs, br, cs_s, cr, ds, dr, es, er, fss, fr, gys, gyr, gzs, gzr, gcs, gcr, sts, st_r, os_, orr) = refs[33:]
+    (s_loc, s_conv, s_turn, s_tok, zs, zr, xs, xr, ags, agr, as_, ar, bs, br, cs_s, cr, ds, dr, es, er, fss, fr, gys, gyr, gzs, gzr, gcs, gcr, sts, st_r, os_, orr) = refs[35:]
     Z, X, Y, TP, FS = g.z, g.x, g.y, g.tp, g.fs
     rows, kb, nb, ffh, ch = g.rows, g.kb, g.nb, g.ffh, g.ch
     TH, R = g.half_rows, g.cell
@@ -117,10 +118,21 @@
     for f_to, t_to in peers:
         pl.semaphore_signal(bar, inc=1, device_id=(f_to, t_to), device_id_type=MESH)
 
+    turned = (4, 5) if g.turn else ()
+
+    def half_of(p, parity):
+        at = pl.ds(pl.multiple_of(parity * ffh, 16), ffh)
+        if p in turned:
+            return TW.at[p - 4, at]
+        return ws[p if p < 3 else p - 1].at[at]
+
+    def stage_turn(n):
+        return pltpu.make_async_copy(ws[3 + n], ST.at[n], s_turn.at[n])
+
     def local_weight(p):
         if p == 3:
             return pltpu.make_async_copy(co, LW.at[3, fs_i, pl.ds(2 * ch, ch)], s_loc.at[p])
-        src = ws[p if p < 3 else p - 1].at[pl.ds(pl.multiple_of(zp * ffh, 16), ffh)]
+        src = half_of(p, zp)
         return pltpu.make_async_copy(src, LW.at[p, fs_i, pl.ds(0, ffh)], s_loc.at[p])
 
     def local_tok(b):
@@ -131,7 +143,10 @@
     for b in range(nb):
         local_tok(b).start()
     for p in range(7):
-        local_weight(p).start()
+        if p in turned:
+            stage_turn(p - 4).start()
+        else:
+            local_weight(p).start()
 
     def local_conv(n):
         return pltpu.make_async_copy((cv, cgate)[n], HID.at[n, pl.ds(0, kb), pl.ds(0, ch)], s_conv.at[n])
@@ -145,7 +160,7 @@
         if p == 3:
             src = dst = LW.at[3, fs_i, pl.ds(0, 3 * ch)]
         else:
-            src = ws[p if p < 3 else p - 1].at[pl.ds(pl.multiple_of(lax.rem(to, 2) * ffh, 16), ffh)]
+            src = half_of(p, lax.rem(to, 2))
             dst = LW.at[p, fs_i, pl.ds(0, ffh)]
         return rcopy(src, dst, zs.at[p, k], zr.at[p, k], to * X + x, tp_i)
 
@@ -191,7 +206,7 @@
 
     def own(p):
         if p < 7:
-            if p != 3:
+            if p != 3 and p not in turned:
                 local_weight(p).wait()
             for dx in range(1, X):
                 xsend(p, 0, dx).start()
@@ -262,6 +277,16 @@
                 LW[p, i, ffh:] = jnp.zeros((g.lw - ffh, kb), BF16)
             return c
         lax.fori_loop(0, FS, zero, 0)
+    for p in turned:
+        n = p - 4
+        stage_turn(n).wait()
+
+        def turn(i, c):
+            at = pl.ds(pl.multiple_of(i * 128, 128), 128)
+            TW[n, at] = ST[n, :, at].T
+            return c
+        lax.fori_loop(0, 2 * ffh // 128, turn, 0)
+        LW[p, fs_i, 0:ffh] = TW[n, pl.ds(pl.multiple_of(zp * ffh, 16), ffh)]
     GB[0:PAD] = jnp.zeros((PAD, ch), F32)
     GB[PAD + rows:] = jnp.zeros((PAD, ch), F32)
     mark("agz")
@@ -850,8 +875,9 @@
 
 
 def per_device(fs, tp, tokens, g0, wg0, wu0, wd0, g1, cv, cgate, ck, cln, co, g2, wg1, wu1, wd1):
-    ws = [wg0.T, wu0.T, wd0, wg1.T, wu1.T, wd1]
     g = Plan(fs, tp, tokens.shape, wd0.shape, co.shape, ck.shape[0])
+    late = [wg1, wu1] if g.turn else [wg1.T, wu1.T]
+    ws = [wg0.T, wu0.T, wd0, *late, wd1]
     gains = [v.reshape(fs, 1, g.kb) for v in (g0, g1, g2)]
     Z, X, Y, TP, FS = g.z, g.x, g.y, g.tp, g.fs
     dma = pltpu.SemaphoreType.DMA
@@ -874,7 +900,9 @@
         vm((8, g.rows), F32),
         vm((TP - 1, 8, g.rows), F32),
         vm((g.rows, 128), F32),
-        dma((7,)), dma((2,)), dma((g.nb,)),
+        vm((2,) + late[0].shape if g.turn else (2, 16, 128), BF16),
+        vm((2,) + late[0].shape[::-1] if g.turn else (2, 16, 128), BF16),
+        dma((7,)), dma((2,)), dma((2,)), dma((g.nb,)),
         dma((7, Z)), dma((7, Z)),
         dma((7, Z, X)), dma((7, FS)),
         dma((1 + 4 * Y,)), dma((1 + 4 * Y,)),

time: 301 us -> 298 us (0.990)
    unnamed x11 -> x5, local copies, waits for them, and re-layouts: 7.82 us -> 5.54 us
where the time goes in v3:
time: 298 us
  Pallas kernels  292 us (98%)
  local copies, waits for them, and re-layouts  5.54 us (2%)
    pallas_call x1, Pallas kernels, per_device(): pl.pallas_call(partial(body, g), out_shape=jax.ShapeDtypeStruct((g.rows,...  292 us

profile of v3, /device:TPU:27, one launch (start us, length us, event | category | flops | bytes accessed | tf_op | source)
XLA Modules:
  0.0 297.7 jit_solution(15038222977238516531)
XLA Ops:
  0.0 0.0 copy-start
  0.0 2.3 copy.16
  2.3 0.0 copy-done
  2.3 1.2 copy.17
  3.5 292.1 %layer.1 = bf16[768,512]{1,0:T(8,128)(2,1)} custom-call(bf16[768,512]{1,0:T(8,128)(2,1)} %refs_0_.1, bf16[1408,256]{1,0:T(8,128)(2,1)} %bitcast.6, bf16[1408,256]{1,0:T(8,128)(2,1)} %bitcast.7, bf16[1408,256]{1,0:T(8,128)(2,1)} %refs_3_.1, bf16[256,1408]{1,0:T(8,128)(2,1)} %refs_4_.1, bf16[256,1408]{1,0:T(8,128)(2,1)} %refs_5_.1, bf16[1408,256]{1,0:T(8,128)(2,1)} %refs_6_.1, ...), custom_call_target="tpu_custom_call" | custom-call | tf_op jit(solution)/shard_map/layer/pallas_call | solution.py:923
  295.6 2.1 copy.19
Async XLA Ops:
  0.0 2.3 copy-start
